TPU v7x, 32 devices: a whole 2x2x4 slice. The times are simulated.
32 devices in a mesh: sp: 8 (over z, x), tp: 4 (over y, core).
Axes of the slice: x: 2, y: 2, z: 4, core: 2. Of those that a mesh axis runs over, the one named last changes fastest.
Arguments:
- residual: bfloat16 [4096, 2048], P('sp'), may hold values from -6 to 6
- queries: bfloat16 [4096, 1024], P('sp', 'tp'), may hold values from -384 to 384
- key_pairs: bfloat16 [4096, 1024], P('sp', 'tp'), may hold values from -384 to 384
- values: bfloat16 [4096, 1024], P('sp', 'tp'), may hold values from -6 to 6
- lambdas: float32 [8], P('tp'), may hold values from 0.3 to 0.8
- head_gain: float32 [128], replicated, may hold values from 0.1 to 1.9
- w_out: bfloat16 [1024, 2048], replicated, may hold values from -0.1875 to 0.1875
- norm_gain: float32 [2048], replicated, may hold values from 0.1 to 1.9
- w_gate: bfloat16 [2048, 5632], P('sp', 'tp'), may hold values from -0.125 to 0.125
- w_up: bfloat16 [2048, 5632], P('sp', 'tp'), may hold values from -0.125 to 0.125
- w_down: bfloat16 [5632, 2048], P('tp', 'sp'), may hold values from -0.078125 to 0.078125
Outputs:
- layer_out: bfloat16 [4096, 2048], P(('sp', 'tp'))
All inputs are finite; a program needn't handle non-finite values.
Results may differ from a plain program's by a relative error of at most 0.018.
Values may be sent and summed in bfloat16 or wider, within the bound.
A program may use at most 128 MiB of HBM per device.

v0:
```python
import math
import jax
import jax.numpy as jnp
from jax import lax
from jax.sharding import PartitionSpec as P

HD = 64


def per_device(
    residual, queries, key_pairs, values, lambdas, head_gain, w_out, norm_gain, w_gate, w_up, w_down
):
    local_rows = queries.shape[0]
    heads_here = lambdas.shape[0]
    value_width = values.shape[1] // heads_here
    score_scale = HD ** (-0.5)
    query_view = queries.reshape(local_rows, heads_here, 2, HD)

    def update(carry, key_block, value_block):
        highest, totals, mixture = carry
        scores = (
            jnp.einsum("qhmd,khmd->hmqk", query_view, key_block, preferred_element_type=jnp.float32)
            * score_scale
        )
        new_high = jnp.maximum(highest, jnp.max(scores, axis=-1))
        shrink = jnp.exp(highest - new_high)
        weights = jnp.exp(scores - new_high[..., None])
        totals = totals * shrink + jnp.sum(weights, axis=-1)
        mixture = mixture * shrink[..., None] + jnp.einsum(
            "hmqk,khe->hmqe",
            weights.astype(jnp.bfloat16),
            value_block,
            preferred_element_type=jnp.float32,
        )
        return (new_high, totals, mixture)

    initial = (
        jnp.full((heads_here, 2, local_rows), -jnp.inf, jnp.float32),
        jnp.zeros((heads_here, 2, local_rows), jnp.float32),
        jnp.zeros((heads_here, 2, local_rows, value_width), jnp.float32),
    )
    key_piece = lax.all_gather(key_pairs, "sp", axis=0, tiled=True)
    value_piece = lax.all_gather(values, "sp", axis=0, tiled=True)
    length = key_piece.shape[0]
    span = math.gcd(length, 512)
    key_blocks = key_piece.reshape(length // span, span, heads_here, 2, HD)
    value_blocks = value_piece.reshape(length // span, span, heads_here, value_width)

    def advance(position, inner):
        return update(inner, key_blocks[position], value_blocks[position])

    highest, totals, mixture = lax.fori_loop(0, length // span, advance, initial)
    mixed = mixture / totals[..., None]
    differ = mixed[:, 0] - lambdas[:, None, None] * mixed[:, 1]
    normed_heads = (
        differ * lax.rsqrt(jnp.mean(differ * differ, axis=-1, keepdims=True) + 1e-05) * head_gain
    )
    heads_out = (
        jnp.transpose(normed_heads, (1, 0, 2))
        .reshape(local_rows, heads_here * value_width)
        .astype(jnp.bfloat16)
    )
    tp_index = lax.axis_index("tp")
    own_rows = local_rows // lax.axis_size("tp")
    own_begin = tp_index * own_rows
    w_mine = lax.dynamic_slice_in_dim(
        w_out, tp_index * heads_here * value_width, heads_here * value_width, 0
    )
    projected = lax.psum_scatter(
        jnp.dot(heads_out, w_mine, preferred_element_type=jnp.float32).astype(jnp.bfloat16),
        "tp",
        scatter_dimension=0,
        tiled=True,
    ).astype(jnp.float32)
    residual_own = lax.dynamic_slice_in_dim(residual, own_begin, own_rows, 0)
    hidden_own = (residual_own.astype(jnp.float32) + projected).astype(jnp.bfloat16)
    stream_f = hidden_own.astype(jnp.float32)
    scaled = stream_f * lax.rsqrt(jnp.mean(stream_f * stream_f, axis=-1, keepdims=True) + 1e-05)
    normed_rows = lax.all_gather(
        (scaled * norm_gain).astype(jnp.bfloat16), "tp", axis=0, tiled=True
    )
    unit_width = w_gate.shape[1]
    joined = jnp.concatenate([w_gate, w_up], axis=1)
    both_sums = jnp.dot(
        normed_rows,
        lax.all_gather(joined, "sp", axis=0, tiled=True),
        preferred_element_type=jnp.float32,
    )
    gate_sum = both_sums[:, :unit_width]
    up_sum = both_sums[:, unit_width:]
    hidden_units = (jax.nn.silu(gate_sum) * up_sum).astype(jnp.bfloat16)
    down_whole = lax.all_gather(w_down, "sp", axis=1, tiled=True)
    ffn_out = lax.psum_scatter(
        jnp.dot(hidden_units, down_whole, preferred_element_type=jnp.float32).astype(jnp.bfloat16),
        "tp",
        scatter_dimension=0,
        tiled=True,
    ).astype(jnp.float32)
    return (hidden_own.astype(jnp.float32) + ffn_out).astype(jnp.bfloat16)


def solution(mesh):
    placed = (
        P("sp", None),
        P("sp", "tp"),
        P("sp", "tp"),
        P("sp", "tp"),
        P("tp"),
        P(),
        P(),
        P(),
        P("sp", "tp"),
        P("sp", "tp"),
        P("tp", "sp"),
    )
    return jax.shard_map(
        per_device, mesh=mesh, in_specs=placed, out_specs=P(("sp", "tp"), None), check_vma=False
    )
```

profile of v0, /device:TPU:0, one launch (start us, length us, event | category | flops | bytes accessed | tf_op | source)
XLA Modules:
  0.0 547.7 jit_solution(14696506700024109413)
XLA Ops:
  9.2 52.1 %all-gather.6.cloned.1.call-done = bf16[4096,256]{1,0:T(8,128)(2,1)} async-done(((bf16[512,256]{1,0:T(8,128)(2,1)}), bf16[4096,256]{1,0:T(8,128)(2,1)}) %all-gather.6.cloned.1.call-update) | async-done | bytes 2097168 | tf_op jit(solution)/shard_map/all_gather | solution.py:42
  61.3 8.3 %reshape.37 = bf16[8,512,2,2,64]{4,3,2,1,0:T(2,128)(2,1)} reshape(bf16[4096,256]{1,0:T(8,128)(2,1)} %all-gather.6.cloned.1.call-done) | data formatting | bytes 4194304 | tf_op jit(solution)/shard_map/reshape | solution.py:46
  69.6 9.1 %copy.19 = bf16[8,512,2,2,64]{1,4,3,2,0:T(8,128)(2,1)S(1)} copy(bf16[8,512,2,2,64]{4,3,2,1,0:T(2,128)(2,1)} %reshape.37) | data formatting | bytes 4194304
  78.7 32.4 %all-gather.8.cloned.1.call-done = bf16[4096,256]{1,0:T(8,128)(2,1)} async-done(((bf16[512,256]{1,0:T(8,128)(2,1)}), bf16[4096,256]{1,0:T(8,128)(2,1)}) %all-gather.8.cloned.1.call-update) | async-done | bytes 2097168 | tf_op jit(solution)/shard_map/all_gather | solution.py:43
  111.1 4.0 reshape.38
  115.0 67.2 %while.18 = (s32[]{:T(128)}, f32[2,2,512]{2,1,0:T(2,128)S(1)}, f32[2,2,512]{2,1,0:T(2,128)S(1)}, f32[2,2,512,128]{3,2,1,0:T(8,128)S(1)}, bf16[8,512,2,2,64]{1,4,...) while((s32[]{:T(128)}, f32[2,2,512]{2,1,0:T(2,128)S(1)}, ...), condition=%wide.region_3.0_spmd.clone, body=%wide.region_0.0_spmd.clone.sunk | while | flops 411838464 | bytes 32899212 | solution.py:52
  115.0 2.7 bitcast_reduce_fusion.2
  117.7 3.0 fusion.44
  123.4 2.7 bitcast_reduce_fusion.2
  126.1 3.0 fusion.44
  131.8 2.7 bitcast_reduce_fusion.2
  134.5 3.0 fusion.44
  140.2 2.7 bitcast_reduce_fusion.2
  142.9 3.0 fusion.44
  148.6 2.7 bitcast_reduce_fusion.2
  151.3 3.0 fusion.44
  157.0 2.7 bitcast_reduce_fusion.2
  159.7 3.0 fusion.44
  165.4 2.7 bitcast_reduce_fusion.2
  168.1 3.0 fusion.44
  173.8 2.7 bitcast_reduce_fusion.2
  176.5 3.0 fusion.44
  183.2 3.3 convolution_convert_fusion
  186.6 29.8 %reduce-scatter.3.cloned.1.call-done = bf16[128,2048]{1,0:T(8,128)(2,1)} async-done(((bf16[512,2048]{1,0:T(8,128)(2,1)}), bf16[128,2048]{1,0:T(8,128)(2,1)}) %reduce-scatter.3.cloned.1.call-update) | async-done | bytes 524304 | tf_op jit(solution)/shard_map/reduce_scatter | solution.py:69
  216.4 1.5 fusion.20
  221.0 20.6 %all-gather.10.cloned.1.call-done = bf16[512,2048]{1,0:T(8,128)(2,1)} async-done(((bf16[128,2048]{1,0:T(8,128)(2,1)}), bf16[512,2048]{1,0:T(8,128)(2,1)}) %all-gather.10.cloned.1.call-update) | async-done | bytes 2097168 | tf_op jit(solution)/shard_map/all_gather | solution.py:79
  241.6 165.4 %all-gather.12.cloned.1.call-done = bf16[2048,2816]{1,0:T(8,128)(2,1)} async-done(((bf16[256,2816]{1,0:T(8,128)(2,1)}), bf16[2048,2816]{1,0:T(8,128)(2,1)}) %all-gather.12.cloned.1.call-update) | async-done | bytes 11534352 | tf_op jit(solution)/shard_map/all_gather | solution.py:86
  407.0 12.5 %fusion.29 = f32[512,2816]{1,0:T(8,128)} fusion(bf16[512,2048]{1,0:T(8,128)(2,1)} %all-gather.10.cloned.1.call-done, bf16[2048,2816]{1,0:T(8,128)(2,1)} %all-gather.12.cloned.1.call-done), kind=kOutput, calls=%fused_computation.48 | convolution fusion | flops 5905580032 | bytes 19398656 | tf_op jit(solution)/shard_map/dot_general | solution.py:84
  419.5 80.7 %all-gather.14.cloned.1.call-done = bf16[1408,2048]{1,0:T(8,128)(2,1)} async-done(((bf16[1408,256]{1,0:T(8,128)(2,1)}), bf16[1408,2048]{1,0:T(8,128)(2,1)}) %all-gather.14.cloned.1.call-update) | async-done | bytes 5767184 | tf_op jit(solution)/shard_map/all_gather | solution.py:92
  500.2 9.1 %convolution_convert_fusion.1 = bf16[512,2048]{1,0:T(8,128)(2,1)} fusion(bf16[1408,2048]{1,0:T(8,128)(2,1)} %all-gather.14.cloned.1.call-done, f32[512,2816]{1,0:T(8,128)} %fusion.29), kind=kOutput, calls=%fused_computation.23 | convolution fusion | flops 2958163968 | bytes 13631488 | tf_op jit(solution)/shard_map/dot_general | solution.py:94
  509.4 29.5 %reduce-scatter.5.cloned.1.call-done = bf16[128,2048]{1,0:T(8,128)(2,1)} async-done(((bf16[512,2048]{1,0:T(8,128)(2,1)}), bf16[128,2048]{1,0:T(8,128)(2,1)}) %reduce-scatter.5.cloned.1.call-update) | async-done | bytes 524304 | tf_op jit(solution)/shard_map/reduce_scatter | solution.py:93
  538.9 2.0 fusion.23
  (93 shorter events, 27.4 us)
Async XLA Ops:
  6.5 54.8 %all-gather.6.cloned.1.call-start = ((), (), s32[]{:S(2)}) async-start(), calls=%async_computation.2 | async-start | bytes 2359296 | tf_op jit(solution)/shard_map/all_gather | solution.py:42
  7.3 103.8 %all-gather.8.cloned.1.call-start = ((), (), s32[]{:S(2)}) async-start(), calls=%async_computation.3 | async-start | bytes 2359296 | tf_op jit(solution)/shard_map/all_gather | solution.py:43
  8.0 208.4 %reduce-scatter.3.cloned.1.call-start = ((), (), s32[]{:S(2)}) async-start(), calls=%async_computation.4 | async-start | bytes 2621440 | tf_op jit(solution)/shard_map/reduce_scatter | solution.py:69
  117.7 4.2 copy-start
  126.1 4.2 copy-start
  134.5 4.2 copy-start
  142.9 4.2 copy-start
  151.3 4.2 copy-start
  159.7 4.2 copy-start
  168.1 4.2 copy-start
  176.5 4.2 copy-start
  182.2 0.7 copy-start.4
  182.2 0.8 copy-start.5
  186.5 31.4 %copy-start.3 = (f32[2048]{0:T(1024)S(1)}, f32[2048]{0:T(1024)}, u32[]{:S(2)}) copy-start(f32[2048]{0:T(1024)} %param.20) | copy-start | bytes 24580
  186.5 32.4 %copy-start.1 = (bf16[256,1408]{1,0:T(8,128)(2,1)S(1)}, bf16[256,1408]{1,0:T(8,128)(2,1)}, u32[]{:S(2)}) copy-start(bf16[256,1408]{1,0:T(8,128)(2,1)} %param.22) | copy-start | bytes 2162692
  186.5 32.4 %copy-start.2 = (bf16[256,1408]{1,0:T(8,128)(2,1)S(1)}, bf16[256,1408]{1,0:T(8,128)(2,1)}, u32[]{:S(2)}) copy-start(bf16[256,1408]{1,0:T(8,128)(2,1)} %param.21) | copy-start | bytes 2162692
  186.6 55.1 %all-gather.10.cloned.1.call-start = ((), (), s32[]{:S(2)}) async-start(), calls=%async_computation.5 | async-start | bytes 2621440 | tf_op jit(solution)/shard_map/all_gather | solution.py:79
  218.9 188.1 %all-gather.12.cloned.1.call-start = ((), (), s32[]{:S(2)}) async-start(), calls=%async_computation.6 | async-start | bytes 12976128 | tf_op jit(solution)/shard_map/all_gather | solution.py:86
  220.2 280.0 %all-gather.14.cloned.1.call-start = ((), (), s32[]{:S(2)}) async-start(), calls=%async_computation.7 | async-start | bytes 6488064 | tf_op jit(solution)/shard_map/all_gather | solution.py:92
  220.8 318.1 %reduce-scatter.5.cloned.1.call-start = ((), (), s32[]{:S(2)}) async-start(), calls=%async_computation.8 | async-start | bytes 2621440 | tf_op jit(solution)/shard_map/reduce_scatter | solution.py:93
Sparse Core Ops, SparseCore 0:
  9.5 51.7 all-gather.5
  63.4 47.6 all-gather.7
  186.7 29.6 reduce-scatter.2
  219.0 22.5 all-gather.9
  243.7 163.2 all-gather.11
  408.9 91.2 all-gather.13
  509.5 29.3 reduce-scatter.4
where the time goes:
time: 548 us
  waiting for transfers between devices  412 us (75%)
  matrix products  57.9 us (11%)
  local copies, waits for them, and re-layouts  32.1 us (6%)
  other arithmetic  30.8 us (6%)
  between operations  13.6 us (2%)
    all_gather x1, waiting for transfers between devices, per_device(): lax.all_gather(joined, 'sp', axis=0, tiled=True)  165 us
    all_gather x1, waiting for transfers between devices, per_device(): down_whole = lax.all_gather(w_down, 'sp', axis=1, tiled=True)  80.7 us
    all_gather x1, waiting for transfers between devices, per_device(): key_piece = lax.all_gather(key_pairs, 'sp', axis=0, tiled=True)  52.1 us
    all_gather x1, waiting for transfers between devices, per_device(): value_piece = lax.all_gather(values, 'sp', axis=0, tiled=True)  32.4 us
    reduce_scatter x1, waiting for transfers between devices, per_device(): lax.psum_scatter(jnp.dot(heads_out, w_mine, preferred_element_type=jnp.fl...  29.8 us
    reduce_scatter x1, waiting for transfers between devices, per_device(): lax.psum_scatter(jnp.dot(hidden_units, down_whole, preferred_element_type...  29.5 us
    reduce_sum x8, other arithmetic, update(): totals = totals * shrink + jnp.sum(weights, axis=-1)  24.3 us
    dot_general x8, matrix products, update(): jnp.einsum('qhmd,khmd->hmqk', query_view, key_block, preferred_element_ty...  21.7 us
  transfers between devices with their start and end apart: 7, of which 7 were waited for; matrix products, arithmetic and copies ran while one was open for 6% of the time, Pallas kernels for 0%

commit v1 on v0

--- a/solution.py
+++ b/solution.py
@@ -39,8 +39,11 @@
         jnp.zeros((heads_here, 2, local_rows), jnp.float32),
         jnp.zeros((heads_here, 2, local_rows, value_width), jnp.float32),
     )
-    key_piece = lax.all_gather(key_pairs, "sp", axis=0, tiled=True)
-    value_piece = lax.all_gather(values, "sp", axis=0, tiled=True)
+    key_piece, value_piece = jnp.split(
+        lax.all_gather(jnp.concatenate([key_pairs, values], axis=1), "sp", axis=0, tiled=True),
+        [key_pairs.shape[1]],
+        axis=1,
+    )
     length = key_piece.shape[0]
     span = math.gcd(length, 512)
     key_blocks = key_piece.reshape(length // span, span, heads_here, 2, HD)

time: 548 us -> 546 us (level)
  waiting for transfers between devices: 412 us -> 402 us
  matrix products: 57.9 us -> 65.5 us
    all_gather x2 -> x1, waiting for transfers between devices: 84.5 us -> 75.4 us  [per_device(): lax.all_gather(jnp.concatenate([key_pairs, values], axis=1), 'sp', axis=0...]
    dot_general x8, matrix products: 21.7 us -> 29.3 us  [update(): jnp.einsum('qhmd,khmd->hmqk', query_view, key_block, preferred_element_ty...]
    unnamed x12 -> x14, local copies, waits for them, and re-layouts: 10.3 us -> 12 us
  transfers between devices with their start and end apart: 7 -> 6, of which waited for: 7 -> 6; matrix products, arithmetic and copies ran while one was open for 6% -> 3% of each run, Pallas kernels for 0% -> 0%
where the time goes in v1:
time: 546 us; the launch traced here: 545 us
  waiting for transfers between devices  402 us (74%)
  matrix products  65.5 us (12%)
  other arithmetic  32.6 us (6%)
  local copies, waits for them, and re-layouts  30.6 us (6%)
  between operations  13.6 us (2%)
    all_gather x1, waiting for transfers between devices, per_device(): lax.all_gather(joined, 'sp', axis=0, tiled=True)  165 us
    all_gather x1, waiting for transfers between devices, per_device(): down_whole = lax.all_gather(w_down, 'sp', axis=1, tiled=True)  80.7 us
    all_gather x1, waiting for transfers between devices, per_device(): lax.all_gather(jnp.concatenate([key_pairs, values], axis=1), 'sp', axis=0...  75.4 us
    reduce_scatter x1, waiting for transfers between devices, per_device(): lax.psum_scatter(jnp.dot(heads_out, w_mine, preferred_element_type=jnp.fl...  29.8 us
    reduce_scatter x1, waiting for transfers between devices, per_device(): lax.psum_scatter(jnp.dot(hidden_units, down_whole, preferred_element_type...  29.5 us
    dot_general x8, matrix products, update(): jnp.einsum('qhmd,khmd->hmqk', query_view, key_block, preferred_element_ty...  29.3 us
    reduce_sum x8, other arithmetic, update(): totals = totals * shrink + jnp.sum(weights, axis=-1)  24.3 us
    all_gather x1, waiting for transfers between devices, per_device(): lax.all_gather((scaled * norm_gain).astype(jnp.bfloat16), 'tp', axis=0, t...  20.8 us
  transfers between devices with their start and end apart: 6, of which 6 were waited for; matrix products, arithmetic and copies ran while one was open for 3% of the time, Pallas kernels for 0%

profile of v1, /device:TPU:0, one launch (start us, length us, event | category | flops | bytes accessed | tf_op | source)
XLA Modules:
  0.0 545.2 jit_solution(14329110708552235107)
XLA Ops:
  6.5 1.9 pad_maximum_fusion.1
  9.6 75.4 %all-gather.5.cloned.1.call-done = bf16[4096,512]{1,0:T(8,128)(2,1)} async-done(((bf16[512,512]{1,0:T(8,128)(2,1)}), bf16[4096,512]{1,0:T(8,128)(2,1)}) %all-gather.5.cloned.1.call-update) | async-done | bytes 4194320 | tf_op jit(solution)/shard_map/all_gather | solution.py:43
  85.0 3.8 fusion.29
  88.8 3.2 reshape.37
  92.1 10.7 %copy.19 = bf16[8,512,2,2,64]{1,4,3,2,0:T(8,128)(2,1)} copy(bf16[8,512,2,2,64]{4,3,2,1,0:T(2,128)(2,1)} %reshape.37) | data formatting | bytes 4194304
  102.8 2.1 reshape.38
  104.9 74.7 %while.18 = (s32[]{:T(128)}, f32[2,2,512]{2,1,0:T(2,128)S(1)}, f32[2,2,512]{2,1,0:T(2,128)S(1)}, f32[2,2,512,128]{3,2,1,0:T(8,128)S(1)}, bf16[8,512,2,2,64]{1,4,...) while((s32[]{:T(128)}, f32[2,2,512]{2,1,0:T(2,128)S(1)}, ...), condition=%wide.region_3.0_spmd.clone, body=%wide.region_0.0_spmd.clone.sunk | while | flops 411838464 | bytes 32899720 | solution.py:55
  104.9 3.7 bitcast_reduce_fusion.2
  108.6 3.0 fusion.45
  114.2 3.7 bitcast_reduce_fusion.2
  117.9 3.0 fusion.45
  123.6 3.7 bitcast_reduce_fusion.2
  127.2 3.0 fusion.45
  132.9 3.7 bitcast_reduce_fusion.2
  136.6 3.0 fusion.45
  142.2 3.7 bitcast_reduce_fusion.2
  145.9 3.0 fusion.45
  151.6 3.7 bitcast_reduce_fusion.2
  155.3 3.0 fusion.45
  160.9 3.7 bitcast_reduce_fusion.2
  164.6 3.0 fusion.45
  170.3 3.7 bitcast_reduce_fusion.2
  174.0 3.0 fusion.45
  180.6 3.3 convolution_convert_fusion
  184.0 29.8 %reduce-scatter.3.cloned.1.call-done = bf16[128,2048]{1,0:T(8,128)(2,1)} async-done(((bf16[512,2048]{1,0:T(8,128)(2,1)}), bf16[128,2048]{1,0:T(8,128)(2,1)}) %reduce-scatter.3.cloned.1.call-update) | async-done | bytes 524304 | tf_op jit(solution)/shard_map/reduce_scatter | solution.py:72
  218.3 20.8 %all-gather.7.cloned.1.call-done = bf16[512,2048]{1,0:T(8,128)(2,1)} async-done(((bf16[128,2048]{1,0:T(8,128)(2,1)}), bf16[512,2048]{1,0:T(8,128)(2,1)}) %all-gather.7.cloned.1.call-update) | async-done | bytes 2097168 | tf_op jit(solution)/shard_map/all_gather | solution.py:82
  239.1 165.4 %all-gather.9.cloned.1.call-done = bf16[2048,2816]{1,0:T(8,128)(2,1)} async-done(((bf16[256,2816]{1,0:T(8,128)(2,1)}), bf16[2048,2816]{1,0:T(8,128)(2,1)}) %all-gather.9.cloned.1.call-update) | async-done | bytes 11534352 | tf_op jit(solution)/shard_map/all_gather | solution.py:89
  404.4 12.5 %fusion.30 = f32[512,2816]{1,0:T(8,128)} fusion(bf16[512,2048]{1,0:T(8,128)(2,1)} %all-gather.7.cloned.1.call-done, bf16[2048,2816]{1,0:T(8,128)(2,1)} %all-gather.9.cloned.1.call-done), kind=kOutput, calls=%fused_computation.50 | convolution fusion | flops 5905580032 | bytes 19398656 | tf_op jit(solution)/shard_map/dot_general | solution.py:87
  417.0 80.7 %all-gather.11.cloned.1.call-done = bf16[1408,2048]{1,0:T(8,128)(2,1)} async-done(((bf16[1408,256]{1,0:T(8,128)(2,1)}), bf16[1408,2048]{1,0:T(8,128)(2,1)}) %all-gather.11.cloned.1.call-update) | async-done | bytes 5767184 | tf_op jit(solution)/shard_map/all_gather | solution.py:95
  497.7 9.1 %convolution_convert_fusion.1 = bf16[512,2048]{1,0:T(8,128)(2,1)} fusion(bf16[1408,2048]{1,0:T(8,128)(2,1)} %all-gather.11.cloned.1.call-done, f32[512,2816]{1,0:T(8,128)} %fusion.30), kind=kOutput, calls=%fused_computation.23 | convolution fusion | flops 2958163968 | bytes 13631488 | tf_op jit(solution)/shard_map/dot_general | solution.py:97
  506.8 29.5 %reduce-scatter.5.cloned.1.call-done = bf16[128,2048]{1,0:T(8,128)(2,1)} async-done(((bf16[512,2048]{1,0:T(8,128)(2,1)}), bf16[128,2048]{1,0:T(8,128)(2,1)}) %reduce-scatter.5.cloned.1.call-update) | async-done | bytes 524304 | tf_op jit(solution)/shard_map/reduce_scatter | solution.py:96
  536.4 2.0 fusion.23
  (94 shorter events, 27.3 us)
Async XLA Ops:
  6.5 78.5 %all-gather.5.cloned.1.call-start = ((), (), s32[]{:S(2)}) async-start(), calls=%async_computation.2 | async-start | bytes 4718592 | tf_op jit(solution)/shard_map/all_gather | solution.py:43
  8.4 205.4 %reduce-scatter.3.cloned.1.call-start = ((), (), s32[]{:S(2)}) async-start(), calls=%async_computation.3 | async-start | bytes 2621440 | tf_op jit(solution)/shard_map/reduce_scatter | solution.py:72
  92.1 10.7 %copy-start.1 = (bf16[4096,256]{1,0:T(8,128)(2,1)S(1)}, bf16[4096,256]{1,0:T(8,128)(2,1)}, u32[]{:S(2)}) copy-start(bf16[4096,256]{1,0:T(8,128)(2,1)} %get-tuple-element.183) | copy-start | bytes 6291460
  108.5 4.2 copy-start
  117.9 4.2 copy-start
  127.2 4.2 copy-start
  136.6 4.2 copy-start
  145.9 4.2 copy-start
  155.3 4.2 copy-start
  164.6 4.2 copy-start
  173.9 4.2 copy-start
  179.6 0.7 copy-start.5
  179.6 0.8 copy-start.6
  183.9 31.4 %copy-start.4 = (f32[2048]{0:T(1024)S(1)}, f32[2048]{0:T(1024)}, u32[]{:S(2)}) copy-start(f32[2048]{0:T(1024)} %param.20) | copy-start | bytes 24580
  183.9 32.5 %copy-start.2 = (bf16[256,1408]{1,0:T(8,128)(2,1)S(1)}, bf16[256,1408]{1,0:T(8,128)(2,1)}, u32[]{:S(2)}) copy-start(bf16[256,1408]{1,0:T(8,128)(2,1)} %param.22) | copy-start | bytes 2162692
  183.9 32.5 %copy-start.3 = (bf16[256,1408]{1,0:T(8,128)(2,1)S(1)}, bf16[256,1408]{1,0:T(8,128)(2,1)}, u32[]{:S(2)}) copy-start(bf16[256,1408]{1,0:T(8,128)(2,1)} %param.21) | copy-start | bytes 2162692
  184.0 55.1 %all-gather.7.cloned.1.call-start = ((), (), s32[]{:S(2)}) async-start(), calls=%async_computation.4 | async-start | bytes 2621440 | tf_op jit(solution)/shard_map/all_gather | solution.py:82
  216.3 188.1 %all-gather.9.cloned.1.call-start = ((), (), s32[]{:S(2)}) async-start(), calls=%async_computation.5 | async-start | bytes 12976128 | tf_op jit(solution)/shard_map/all_gather | solution.py:89
  217.7 280.0 %all-gather.11.cloned.1.call-start = ((), (), s32[]{:S(2)}) async-start(), calls=%async_computation.6 | async-start | bytes 6488064 | tf_op jit(solution)/shard_map/all_gather | solution.py:95
  218.3 318.1 %reduce-scatter.5.cloned.1.call-start = ((), (), s32[]{:S(2)}) async-start(), calls=%async_computation.7 | async-start | bytes 2621440 | tf_op jit(solution)/shard_map/reduce_scatter | solution.py:96
Sparse Core Ops, SparseCore 0:
  9.5 75.4 all-gather.4
  184.1 29.7 reduce-scatter.2
  216.5 22.5 all-gather.6
  241.1 163.2 all-gather.8
  406.3 91.2 all-gather.10
  507.0 29.3 reduce-scatter.4
